TPU v7x, 32 devices: a whole 2x2x4 slice. The times are simulated.
32 devices in a mesh: sp: 16 (over z, y, x), tp: 2 (over core).
Axes of the slice: x: 2, y: 2, z: 4, core: 2. Of those that a mesh axis runs over, the one named last changes fastest.
Arguments:
- resid: bfloat16 [4096, 2048], P(('sp', 'tp')), may hold values from -6 to 6
- queries: bfloat16 [4096, 2048], P('sp', 'tp'), may hold values from -6 to 6
- keys: bfloat16 [4096, 1024], P('sp', 'tp'), may hold values from -6 to 6
- values: bfloat16 [4096, 1024], P('sp', 'tp'), may hold values from -6 to 6
- log_gates: float32 [16, 4096], P('tp'), as said below
- documents: int32 [4096], P('sp'), may hold values from 0 to 2, never falling along the last dimension, each value on 1 to 3072 neighbouring positions
- out_weight: bfloat16 [2048, 2048], P('tp'), may hold values from -0.125 to 0.125
- attn_gain: float32 [2048], replicated, may hold values from 0.1 to 1.9
- mlp_gain: float32 [2048], replicated, may hold values from 0.1 to 1.9
- gate_weight: bfloat16 [2048, 4096], P('sp', 'tp'), may hold values from -0.125 to 0.125
- up_weight: bfloat16 [2048, 4096], P('sp', 'tp'), may hold values from -0.125 to 0.125
- down_weight: bfloat16 [4096, 2048], P('tp', 'sp'), may hold values from -0.375 to 0.375
Outputs:
- mixed: bfloat16 [4096, 2048], P(('sp', 'tp'))
Inputs may be any that keep to these rules, and one draw needn't show every extreme that they name: `log_gates`: each head's row never rises from one position to the next and starts at or below 0. `documents`: document numbers never fall along the positions; one document spans exactly three quarters of the 4096 positions.
All inputs are finite; a program needn't handle non-finite values.
Results may differ from a plain program's by a relative error of at most 0.018.
Values may be sent and summed in bfloat16 or wider, within the bound.
A program may use at most 64 MiB of HBM per device.

v0:
```python
import functools
import math

import jax
import jax.numpy as jnp
from jax import lax
from jax.experimental import pallas as pl
from jax.experimental.pallas import tpu as pltpu
from jax.sharding import PartitionSpec as P

HD = 128


def local(
    resid,
    queries,
    keys,
    values,
    log_gates,
    documents,
    out_weight,
    attn_gain,
    mlp_gain,
    gate_weight,
    up_weight,
    down_weight,
):
    tok_rows = queries.shape[0]
    kv_dev = keys.shape[1] // HD
    heads_dev = log_gates.shape[0]
    group_size = heads_dev // kv_dev
    score_scale = 1.0 / math.sqrt(HD)
    own_start = lax.axis_index("sp") * tok_rows
    own_last = own_start + tok_rows - 1
    first_doc = documents[0]
    query_pos = own_start + lax.iota(jnp.int32, tok_rows)
    query_heads = queries.reshape(tok_rows, kv_dev, group_size, HD)
    key_gates_all = log_gates.reshape(kv_dev, group_size, log_gates.shape[1])
    query_gates = lax.dynamic_slice_in_dim(key_gates_all, own_start, tok_rows, 2)
    collected = (
        lax.all_gather(gate_weight, "sp", axis=0, tiled=True),
        lax.all_gather(up_weight, "sp", axis=0, tiled=True),
        lax.all_gather(down_weight, "sp", axis=1, tiled=True),
    )
    residual_rows = resid.astype(jnp.float32)

    def attend_block(running, key_rows, value_rows, doc_rows, first_row):
        run_max, run_sum, accumulated = running
        key_count = key_rows.shape[0]
        scores = (
            jnp.einsum(
                "tkgd,skd->kgts",
                query_heads,
                key_rows.reshape(key_count, kv_dev, HD),
                preferred_element_type=jnp.float32,
            )
            * score_scale
        )
        key_gates = lax.dynamic_slice_in_dim(key_gates_all, first_row, key_count, 2)
        scores = scores + query_gates[..., None] - key_gates[:, :, None, :]
        key_pos = first_row + lax.iota(jnp.int32, key_count)
        visible = (key_pos[None, :] <= query_pos[:, None]) & (
            doc_rows[None, :] == documents[:, None]
        )
        scores = jnp.where(visible, scores, jnp.float32(-1e30))
        new_max = jnp.maximum(run_max, jnp.max(scores, axis=-1))
        probs = jnp.where(visible, jnp.exp(scores - new_max[..., None]), jnp.float32(0.0))
        shrink = jnp.exp(run_max - new_max)
        run_sum = run_sum * shrink + jnp.sum(probs, axis=-1)
        weighted = jnp.einsum(
            "kgts,skd->kgtd",
            probs.astype(jnp.bfloat16),
            value_rows.reshape(key_count, kv_dev, HD),
            preferred_element_type=jnp.float32,
        )
        accumulated = accumulated * shrink[..., None] + weighted
        return (new_max, run_sum, accumulated)

    def maybe_attend(running, key_rows, value_rows, doc_rows, first_row):
        needed = (first_row <= own_last) & (doc_rows[-1] >= first_doc)

        def compute(state):
            return attend_block(state, key_rows, value_rows, doc_rows, first_row)

        def keep(state):
            return state

        return lax.cond(needed, compute, keep, running)

    start_state = (
        jnp.full((kv_dev, group_size, tok_rows), -1e30, jnp.float32),
        jnp.zeros((kv_dev, group_size, tok_rows), jnp.float32),
        jnp.zeros((kv_dev, group_size, tok_rows, HD), jnp.float32),
    )
    key_rows = lax.all_gather(keys, "sp", axis=0, tiled=True)
    value_rows = lax.all_gather(values, "sp", axis=0, tiled=True)
    doc_rows = lax.all_gather(documents, "sp", axis=0, tiled=True)
    key_count = key_rows.shape[0]
    block_len = math.gcd(key_count, 1024)

    def advance(block_index, inner):
        offset = block_index * block_len
        return maybe_attend(
            inner,
            lax.dynamic_slice_in_dim(key_rows, offset, block_len, 0),
            lax.dynamic_slice_in_dim(value_rows, offset, block_len, 0),
            lax.dynamic_slice_in_dim(doc_rows, offset, block_len, 0),
            offset,
        )

    run_max, run_sum, accumulated = lax.fori_loop(0, key_count // block_len, advance, start_state)
    attended = accumulated / run_sum[..., None]
    attended = (
        jnp.transpose(attended, (2, 0, 1, 3)).reshape(tok_rows, heads_dev * HD).astype(jnp.bfloat16)
    )
    rows_slice = attended
    projected = lax.psum_scatter(
        jnp.dot(rows_slice, out_weight, preferred_element_type=jnp.float32).astype(jnp.bfloat16),
        "tp",
        scatter_dimension=0,
        tiled=True,
    ).astype(jnp.float32)
    power = jnp.mean(projected * projected, axis=-1, keepdims=True)
    middle = residual_rows + attn_gain * projected * lax.rsqrt(power + 1e-06)
    middle_power = jnp.mean(middle * middle, axis=-1, keepdims=True)
    normed = (mlp_gain * middle * lax.rsqrt(middle_power + 1e-06)).astype(jnp.bfloat16)
    normed_all = lax.all_gather(normed, "tp", axis=0, tiled=True)
    gate_full, up_full, down_full = collected
    gate_act = jnp.dot(normed_all, gate_full, preferred_element_type=jnp.float32)
    up_act = jnp.dot(normed_all, up_full, preferred_element_type=jnp.float32)
    hidden = (jax.nn.silu(gate_act) * up_act).astype(jnp.bfloat16)
    rows_slice = hidden
    lowered = lax.psum_scatter(
        jnp.dot(rows_slice, down_full, preferred_element_type=jnp.float32).astype(jnp.bfloat16),
        "tp",
        scatter_dimension=0,
        tiled=True,
    ).astype(jnp.float32)
    return (middle + 0.5 * lowered).astype(jnp.bfloat16)


GROUP = 4
MESH = pl.DeviceIdType.MESH
LOG2E = 1.4426950408889634
VMEM = pl.BlockSpec(memory_space=pltpu.VMEM)


def greet(targets):
    barrier = pltpu.get_barrier_semaphore()
    for target in targets:
        pl.semaphore_signal(barrier, inc=1, device_id=target, device_id_type=MESH)
    pl.semaphore_wait(barrier, len(targets))


def remote(src, dst, send_sem, recv_sem, target):
    return pltpu.make_async_remote_copy(
        src_ref=src,
        dst_ref=dst,
        send_sem=send_sem,
        recv_sem=recv_sem,
        device_id=target,
        device_id_type=MESH,
    )


def spread_kernel(
    plane, q_ref, k_ref, v_ref, d_ref, g_ref, u_ref, w_ref,
    qo, ko, vo, do, go, uo, wo,
    z_send, p_send, recv, q_send, q_recv, local_sem,
):
    me = lax.axis_index("sp")
    core = lax.axis_index("tp")
    z, p = me // plane, me % plane
    rows = k_ref.shape[0]
    qcols = q_ref.shape[1] // GROUP
    fcols = g_ref.shape[1] // GROUP

    def cols(width, index):
        return pl.ds(pl.multiple_of(index * width, width), width)

    def place(a, k):
        if a == 0:
            return ko.at[cols(rows, k)]
        if a == 1:
            return vo.at[cols(rows, k)]
        if a == 2:
            return do.at[k]
        if a == 3:
            return go.at[cols(g_ref.shape[0], k)]
        return (uo, wo)[a - 4].at[k // plane]

    def piece(a, to):
        if a == 0:
            return k_ref.at[:, cols(HD, to)]
        if a == 1:
            return v_ref.at[:, cols(HD, to)]
        if a == 2:
            return d_ref.at[...]
        if a == 3:
            return g_ref.at[:, cols(fcols, to)]
        if a == 4:
            return u_ref.at[:, cols(fcols, to)]
        return w_ref.at[cols(fcols, to)]

    z_peers = [(z + d) % GROUP for d in range(1, GROUP)]
    p_peers = [(p + d) % plane for d in range(1, plane)]
    greet([(t * plane + p, core) for t in z_peers] + [(z * plane + t, core) for t in p_peers])
    waits = []
    keeps = []

    def send_z(a):
        for d in range(1, GROUP):
            to = (z + d) % GROUP
            copy = remote(piece(a, to), place(a, me), z_send.at[a, d - 1],
                          recv.at[a, d, 0], (to * plane + p, core))
            copy.start()
            waits.append(copy)
        own = pltpu.make_async_copy(piece(a, z), place(a, me), local_sem.at[a])
        own.start()
        keeps.append(own)

    def forward(a, dz):
        zs = (z + GROUP - dz) % GROUP
        at = place(a, zs * plane + p)
        if dz:
            remote(at, at, z_send.at[a, dz - 1], recv.at[a, dz, 0], (me, core)).wait_recv()
        else:
            keeps[a].wait()
        for e in range(1, plane):
            copy = remote(at, at, p_send.at[a, dz, e - 1], recv.at[a, dz, e],
                          (z * plane + (p + e) % plane, core))
            copy.start()
            waits.append(copy)

    for a in (0, 1, 2):
        send_z(a)
    for d in range(1, GROUP):
        to = (z + d) % GROUP
        copy = remote(q_ref.at[:, cols(qcols, to)], qo.at[z], q_send.at[d - 1],
                      q_recv.at[d - 1], (to * plane + p, core))
        copy.start()
        waits.append(copy)
    own_q = pltpu.make_async_copy(q_ref.at[:, cols(qcols, z)], qo.at[z], local_sem.at[6])
    own_q.start()
    for a in (3, 4, 5):
        send_z(a)
    for group in ((0, 1, 2), (3,)):
        for dz in (0, 1, 3, 2):
            for a in group:
                forward(a, dz)
    for a in (4, 5):
        keeps[a].wait()
        for d in range(1, GROUP):
            at = place(a, ((z + GROUP - d) % GROUP) * plane + p)
            remote(at, at, z_send.at[a, d - 1], recv.at[a, d, 0], (me, core)).wait_recv()
    own_q.wait()
    for copy in waits:
        copy.wait_send()
    for d in range(1, GROUP):
        at = qo.at[(z + GROUP - d) % GROUP]
        remote(at, at, q_send.at[d - 1], q_recv.at[d - 1], (me, core)).wait_recv()
    for a in range(4):
        for dz in range(GROUP):
            zs = (z + GROUP - dz) % GROUP
            for e in range(1, plane):
                at = place(a, zs * plane + (p + plane - e) % plane)
                remote(at, at, p_send.at[a, dz, e - 1], recv.at[a, dz, e], (me, core)).wait_recv()


def attend_kernel(lo_ref, hi_ref, q_ref, k_ref, v_ref, gq_ref, gk_ref, dq_ref, dk_ref, pos_ref,
                  out_ref):
    block = 512
    rows = q_ref.shape[1]
    rank = q_ref.shape[2] // HD
    coef = LOG2E / math.sqrt(HD)

    def one(b, carry):
        q = jnp.concatenate([q_ref[b, :, r * HD:(r + 1) * HD] for r in range(rank)], axis=0)
        dq = dq_ref[b]
        qpos = pos_ref[b]
        gq = gq_ref[b]

        def step(i, state):
            m, l, acc = state
            at = pl.ds(pl.multiple_of(i * block, block), block)
            s = lax.dot_general(q, k_ref[at], (((1,), (1,)), ((), ())),
                                preferred_element_type=jnp.float32)
            gk = jnp.concatenate(
                [jnp.broadcast_to(gk_ref[r:r + 1, at], (rows, block)) for r in range(rank)], axis=0)
            s = s * coef + (gq - gk)
            kpos = i * block + lax.broadcasted_iota(jnp.int32, (1, block), 1)
            seen = (kpos <= qpos) & (dk_ref[0:1, at] == dq)
            s = jnp.where(seen, s, jnp.float32(-1e30))
            m_new = jnp.maximum(m, jnp.max(s, axis=1, keepdims=True))
            prob = jnp.exp2(s - m_new)
            shrink = jnp.exp2(m - m_new)
            l = l * shrink + jnp.sum(prob, axis=1, keepdims=True)
            acc = acc * shrink + jnp.dot(prob.astype(jnp.bfloat16), v_ref[at],
                                         preferred_element_type=jnp.float32)
            return m_new, l, acc

        start = (jnp.full((rank * rows, 1), -1e20, jnp.float32),
                 jnp.zeros((rank * rows, 1), jnp.float32),
                 jnp.zeros((rank * rows, HD), jnp.float32))
        m, l, acc = lax.fori_loop(lo_ref[b], hi_ref[b], step, start)
        res = (acc / l).astype(jnp.bfloat16)
        for r in range(rank):
            out_ref[b, :, r * HD:(r + 1) * HD] = res[r * rows:(r + 1) * rows]
        return carry

    lax.fori_loop(0, q_ref.shape[0], one, 0)


def finish_kernel(
    plane, att_ref, ow_ref, resid_ref, ag_ref, mg_ref, gw, uz_ref, wz_ref, out_ref,
    uw, dw, arr, pbuf, pgot, mid, nall, hid, part, pair, red, got,
    a_send, a_recv, t_send, t_recv, o_send, n_send, n_recv, f_send, f_recv,
    x_send, x_recv, r_send, r_recv, w_send, w_recv, w_local, local_sem,
):
    me = lax.axis_index("sp")
    core = lax.axis_index("tp")
    z, p = me // plane, me % plane
    other = 1 - core
    mate = (me, other)
    width = att_ref.shape[2]
    half = resid_ref.shape[0]
    d_model = resid_ref.shape[1]
    wrows, wcols = uz_ref.shape[1], wz_ref.shape[2]
    tile = 512

    def there(d):
        return (((z + d) % GROUP) * plane + p, core)

    def near(e):
        return (z * plane + (p + e) % plane, core)

    def weight(a, k):
        if a == 0:
            return uw.at[pl.ds(pl.multiple_of(k * wrows, wrows), wrows)]
        return dw.at[:, pl.ds(pl.multiple_of(k * wcols, wcols), wcols)]

    greet([there(d) for d in range(1, GROUP)] + [near(e) for e in range(1, plane)] + [mate])
    for d in range(1, GROUP):
        remote(att_ref.at[(z + d) % GROUP], arr.at[z], a_send.at[d - 1], a_recv.at[d - 1],
               there(d)).start()
    own = pltpu.make_async_copy(att_ref.at[z], arr.at[z], local_sem)
    own.start()
    staged = (uz_ref, wz_ref)
    for a in range(2):
        for g in range(GROUP):
            at = weight(a, g * plane + p)
            pltpu.make_async_copy(staged[a].at[g], at, w_local.at[a, g]).start()
            for e in range(1, plane):
                remote(staged[a].at[g], at, w_send.at[a, g, e - 1], w_recv.at[a, g, e - 1],
                       near(e)).start()
    own.wait()
    for d in range(1, GROUP):
        at = arr.at[(z + GROUP - d) % GROUP]
        remote(at, at, a_send.at[d - 1], a_recv.at[d - 1], mate).wait_recv()

    @pl.loop(0, d_model // tile)
    def _(j):
        at = pl.ds(pl.multiple_of(j * tile, tile), tile)
        total = jnp.dot(arr[0], ow_ref[0:width, at], preferred_element_type=jnp.float32)
        for g in range(1, GROUP):
            total += jnp.dot(arr[g], ow_ref[g * width:(g + 1) * width, at],
                             preferred_element_type=jnp.float32)
        pbuf[0, :, at] = total[:half].astype(jnp.bfloat16)
        pbuf[1, :, at] = total[half:].astype(jnp.bfloat16)

    swap = remote(pbuf.at[other], pgot, t_send, t_recv, mate)
    swap.start()
    swap.wait()
    projected = pbuf[core].astype(jnp.float32) + pgot[...].astype(jnp.float32)
    power = jnp.mean(projected * projected, axis=-1, keepdims=True)
    middle = resid_ref[...].astype(jnp.float32) + ag_ref[...] * projected * lax.rsqrt(power + 1e-06)
    mid[...] = middle
    mpower = jnp.mean(middle * middle, axis=-1, keepdims=True)
    nall[z, core] = (mg_ref[...] * middle * lax.rsqrt(mpower + 1e-06)).astype(jnp.bfloat16)

    def relay(zb, side, send_sem):
        block = nall.at[zb, core]
        return remote(block, block, send_sem, n_recv.at[zb],
                      ((z + 1 - 2 * side) * plane + p, core))

    def share(zb):
        block = nall.at[zb, core]
        return remote(block, block, f_send.at[zb], f_recv.at[zb], mate)

    def onward(side):
        return (side == 0) & (z < GROUP - 1) | (side == 1) & (z > 0)

    for side in (0, 1):
        @pl.when(onward(side))
        def _():
            relay(z, side, o_send.at[side]).start()
    share(z).start()

    def feed(zb):
        over = nall.at[zb, other]
        remote(over, over, f_send.at[zb], f_recv.at[zb], mate).wait_recv()
        rows_in = jnp.concatenate([nall[zb, 0], nall[zb, 1]], axis=0)
        ftile = 256
        for j in range(hid.shape[1] // ftile):
            at = slice(j * ftile, (j + 1) * ftile)
            gate = jnp.dot(rows_in, gw[:, at], preferred_element_type=jnp.float32)
            up = jnp.dot(rows_in, uw[:, at], preferred_element_type=jnp.float32)
            hid[:, at] = (gate / (1.0 + jnp.exp(-gate)) * up).astype(jnp.bfloat16)

        @pl.loop(0, d_model // tile)
        def _(j):
            at = pl.ds(pl.multiple_of(j * tile, tile), tile)
            total = jnp.dot(hid[...], dw[:, at], preferred_element_type=jnp.float32)
            part[zb, 0, :, at] = total[:half].astype(jnp.bfloat16)
            part[zb, 1, :, at] = total[half:].astype(jnp.bfloat16)

        trade = remote(part.at[zb, other], pair.at[zb], x_send.at[zb], x_recv.at[zb], mate)
        trade.start()
        trade.wait()
        return part[zb, core].astype(jnp.float32) + pair[zb].astype(jnp.float32)

    def arrive(d):
        for side in (0, 1):
            zb = z - d if side == 0 else z + d

            @pl.when((zb >= 0) & (zb < GROUP))
            def _():
                block = nall.at[zb, core]
                remote(block, block, n_send.at[zb], n_recv.at[zb], mate).wait_recv()
                @pl.when(onward(side))
                def _():
                    relay(zb, side, n_send.at[zb]).start()
                share(zb).start()

    arrive(1)
    arrive(2)
    for a in range(2):
        for g in range(GROUP):
            pltpu.make_async_copy(staged[a].at[g], weight(a, g * plane + p),
                                  w_local.at[a, g]).wait()
            for e in range(1, plane):
                at = weight(a, g * plane + (p + plane - e) % plane)
                remote(staged[a].at[g], at, w_send.at[a, g, e - 1], w_recv.at[a, g, e - 1],
                       near(e)).wait()
    for d in (2, 1, 3):
        if d == 3:
            arrive(d)

        @pl.loop(0, 2)
        def _(side):
            zb = z + (2 * side - 1) * d

            @pl.when((zb >= 0) & (zb < GROUP))
            def _():
                red[zb] = feed(zb).astype(jnp.bfloat16)
                remote(red.at[zb], got.at[z], r_send.at[zb], r_recv.at[z],
                       (zb * plane + p, core)).start()
    total = mid[...] + 0.5 * feed(z)
    for d in range(1, GROUP):
        zb = (z + d) % GROUP
        remote(red.at[zb], got.at[zb], r_send.at[zb], r_recv.at[zb], mate).wait()
        total += 0.5 * got[zb].astype(jnp.float32)
    out_ref[...] = total.astype(jnp.bfloat16)
    share(z).wait_send()
    for side in (0, 1):
        @pl.when(onward(side))
        def _():
            relay(z, side, o_send.at[side]).wait_send()
    for d in range(1, GROUP):
        remote(att_ref.at[0], arr.at[0], a_send.at[d - 1], a_recv.at[d - 1], mate).wait_send()
        share((z + d) % GROUP).wait_send()
        for side in (0, 1):
            zb = z - d if side == 0 else z + d

            @pl.when((zb >= 0) & (zb < GROUP) & onward(side))
            def _():
                relay(zb, side, n_send.at[zb]).wait_send()


def grouped(
    sp, resid, queries, keys, values, log_gates, documents, out_weight, attn_gain, mlp_gain,
    gate_weight, up_weight, down_weight,
):
    plane = sp // GROUP
    rows, ff = keys.shape[0], gate_weight.shape[1] // GROUP
    d_model = resid.shape[1]
    wrows, wcols = gate_weight.shape[0], down_weight.shape[1]
    tokens = rows * sp
    qcols = queries.shape[1] // GROUP
    rank = qcols // HD
    bf = jnp.bfloat16
    me = lax.axis_index("sp")
    z, p = me // plane, me % plane
    shape = jax.ShapeDtypeStruct
    dma = pltpu.SemaphoreType.DMA
    limit = 60 * 1024 * 1024
    q4, k_all, v_all, docs, g_all, u_all, w_all = pl.pallas_call(
        functools.partial(spread_kernel, plane),
        out_shape=(
            shape((GROUP, rows, qcols), bf), shape((tokens, HD), bf), shape((tokens, HD), bf),
            shape((sp, 8, rows), jnp.int32),
            shape((d_model, ff), bf), shape((GROUP, wrows, ff), bf),
            shape((GROUP, ff, wcols), bf),
        ),
        in_specs=[VMEM] * 7,
        out_specs=[VMEM] * 7,
        scratch_shapes=[
            dma((6, GROUP - 1)), dma((6, GROUP, plane - 1)), dma((6, GROUP, plane)),
            dma((GROUP - 1,)), dma((GROUP - 1,)), dma((7,)),
        ],
        compiler_params=pltpu.CompilerParams(
            collective_id=0, has_side_effects=True, vmem_limit_bytes=limit),
    )(queries, keys, values, jnp.broadcast_to(documents[None, :], (8, rows)),
      gate_weight, up_weight, down_weight)

    docs_all = docs[:, 0, :].reshape(tokens)
    gates = lax.dynamic_slice_in_dim(log_gates, z * rank, rank, 0) * LOG2E
    def mine(x):
        return lax.dynamic_index_in_dim(x, p, x.ndim - 2, keepdims=False)
    gq = mine(gates.reshape(rank, GROUP, plane, rows))
    gq = jnp.transpose(gq, (1, 0, 2)).reshape(GROUP, rank * rows, 1)
    dq = mine(docs_all.reshape(GROUP, plane, rows))
    pos = mine(lax.iota(jnp.int32, tokens).reshape(GROUP, plane, rows))
    block = 512
    hi = (pos[:, -1] + block) // block
    lo = jnp.sum((docs_all[None, :] < dq[:, :1]).astype(jnp.int32), axis=1) // block
    SMEM = pl.BlockSpec(memory_space=pltpu.SMEM)
    attended = pl.pallas_call(
        attend_kernel,
        out_shape=shape((GROUP, rows, qcols), bf),
        in_specs=[SMEM, SMEM] + [VMEM] * 8,
        out_specs=VMEM,
        compiler_params=pltpu.CompilerParams(vmem_limit_bytes=limit),
    )(lo, hi, q4, k_all, v_all, gq, gates, jnp.tile(dq, (1, rank))[..., None],
      docs_all[None, :], jnp.tile(pos, (1, rank))[..., None])

    half = resid.shape[0]
    return pl.pallas_call(
        functools.partial(finish_kernel, plane),
        out_shape=shape(resid.shape, bf),
        in_specs=[VMEM] * 8,
        out_specs=VMEM,
        scratch_shapes=[
            pltpu.VMEM((d_model, ff), bf),
            pltpu.VMEM((ff, d_model), bf),
            pltpu.VMEM((GROUP, rows, qcols), bf),
            pltpu.VMEM((2, half, d_model), bf),
            pltpu.VMEM((half, d_model), bf),
            pltpu.VMEM((half, d_model), jnp.float32),
            pltpu.VMEM((GROUP, 2, half, d_model), bf),
            pltpu.VMEM((rows, ff), bf),
            pltpu.VMEM((GROUP, 2, half, d_model), bf),
            pltpu.VMEM((GROUP, half, d_model), bf),
            pltpu.VMEM((GROUP, half, d_model), bf),
            pltpu.VMEM((GROUP, half, d_model), bf),
            dma((GROUP - 1,)), dma((GROUP - 1,)), dma, dma,
            dma((2,)), dma((GROUP,)), dma((GROUP,)), dma((GROUP,)), dma((GROUP,)),
            dma((GROUP,)), dma((GROUP,)), dma((GROUP,)), dma((GROUP,)),
            dma((2, GROUP, plane - 1)), dma((2, GROUP, plane - 1)), dma((2, GROUP)), dma,
        ],
        compiler_params=pltpu.CompilerParams(
            collective_id=1, has_side_effects=True, vmem_limit_bytes=limit),
    )(attended, out_weight, resid, attn_gain[None, :], mlp_gain[None, :], g_all, u_all, w_all)


def solution(mesh):
    placed = (
        P(("sp", "tp"), None),
        P("sp", "tp"),
        P("sp", "tp"),
        P("sp", "tp"),
        P("tp", None),
        P("sp"),
        P("tp", None),
        P(),
        P(),
        P("sp", "tp"),
        P("sp", "tp"),
        P("tp", "sp"),
    )
    sp, tp = mesh.shape["sp"], mesh.shape["tp"]

    def layer(*args):
        kv_dev = args[2].shape[1] // HD
        fits = tp == 2 and sp % GROUP == 0 and kv_dev == GROUP
        return grouped(sp, *args) if fits else local(*args)

    return jax.shard_map(
        layer, mesh=mesh, in_specs=placed, out_specs=P(("sp", "tp"), None), check_vma=False
    )
```

profile of v0, /device:TPU:10, one launch (start us, length us, event | category | flops | bytes accessed | tf_op | source)
XLA Modules:
  0.0 202.9 jit_solution(17740857426327447986)
XLA Ops:
  0.0 1.3 broadcast_in_dim.12.d_ref
  1.3 0.9 dynamic-slice_multiply_fusion.gk_ref
  2.2 0.0 copy-start
  2.3 0.1 copy.26
  2.4 1.9 tile.21.pos_ref
  4.3 1.4 copy.27.gq_ref
  5.7 68.8 %shard_map.118 = (bf16[4,256,256]{2,1,0:T(8,128)(2,1)}, bf16[4096,128]{1,0:T(8,128)(2,1)}, bf16[4096,128]{1,0:T(8,128)(2,1)}, s32[16,8,256]{2,1,0:T(8,128)}, bf1...) custom-call(bf16[256,1024]{1,0:T(8,128)(2,1)} %q_ref.1, ...), custom_call_target="tpu_custom_call" | custom-call | tf_op jit(solution)/shard_map/pallas_call | solution.py:497
  74.5 1.0 slice_reduce_fusion
  75.5 0.0 copy-start.1
  75.5 0.1 copy.23
  75.7 0.1 copy.25
  75.8 0.2 convert_reduce_fusion
  76.0 0.6 and_select_fusion
  76.6 1.9 tile.20.dq_ref
  78.5 0.0 copy-done
  78.5 0.0 copy-done.1
  78.5 14.0 %shard_map.119.att_ref = bf16[4,256,256]{2,1,0:T(8,128)(2,1)} custom-call(s32[4]{0:T(128)} %get-tuple-element.22.lo_ref, s32[4]{0:T(128)} %get-tuple-element.21.hi_ref, bf16[4,256,256]{2,1,0:T(8,128)(2,1)} %get-tuple-element.13.q_ref, bf16[4096,128]{1,0:T(8,128)(2,1)} %get-tuple-element.14.k_ref, bf16[4096,128]{1,0:T(8,128)(2,1)} %get-tuple-element.15.v_ref, ...), custom_call_target="tpu_custom_call" | custom-call | tf_op jit(solution)/shard_map/pallas_call | solution.py:528
  92.5 108.6 %shard_map.120 = bf16[128,2048]{1,0:T(8,128)(2,1)} custom-call(bf16[4,256,256]{2,1,0:T(8,128)(2,1)} %shard_map.119.att_ref, bf16[1024,2048]{1,0:T(8,128)(2,1)} %ow_ref.1, bf16[128,2048]{1,0:T(8,128)(2,1)} %resid_ref.1, f32[1,2048]{1,0:T(1,128)} %bitcast.23, f32[1,2048]{1,0:T(1,128)} %bitcast.24, bf16[2048,512]{1,0:T(8,128)(2,1)} %get-tuple-element.16.gw, ...), custom_call_target="tpu_custom_call" | custom-call | tf_op jit(solution)/shard_map/pallas_call | solution.py:538
  201.1 1.9 copy.33
  (9 shorter events, 0.1 us)
Async XLA Ops:
  2.2 76.3 %copy-start = (f32[2,4096]{1,0:T(2,128)}, f32[2,4096]{1,0:T(2,128)S(1)}, u32[]{:S(2)}) copy-start(f32[2,4096]{1,0:T(2,128)S(1)} %dynamic-slice_multiply_fusion.gk_ref) | copy-start | bytes 98308
  75.5 3.0 %copy-start.1 = (s32[16,1,256]{2,1,0:T(1,128)}, s32[16,1,256]{2,1,0:T(1,128)S(1)}, u32[]{:S(2)}) copy-start(s32[16,1,256]{2,1,0:T(1,128)S(1)} %get-tuple-element.20) | copy-start | bytes 49156
where the time goes:
time: 203 us
  Pallas kernels  191 us (94%)
  local copies, waits for them, and re-layouts  9.73 us (5%)
    pallas_call x1, Pallas kernels, grouped(): pl.pallas_call(functools.partial(finish_kernel, plane), out_shape=shape(r...  109 us
    pallas_call x1, Pallas kernels, grouped(): pl.pallas_call(functools.partial(spread_kernel, plane), out_shape=(shape(...  68.8 us
    pallas_call x1, Pallas kernels, grouped(): pl.pallas_call(attend_kernel, out_shape=shape((GROUP, rows, qcols), bf),...  14 us

commit v1 on v0

v1 whole, which is shorter than its diff:
```python
import math

import jax
import jax.numpy as jnp
from jax import lax
from jax.experimental import pallas as pl
from jax.experimental.pallas import tpu as pltpu
from jax.sharding import PartitionSpec as P

HD = 128


def local(
    resid,
    queries,
    keys,
    values,
    log_gates,
    documents,
    out_weight,
    attn_gain,
    mlp_gain,
    gate_weight,
    up_weight,
    down_weight,
):
    tok_rows = queries.shape[0]
    kv_dev = keys.shape[1] // HD
    heads_dev = log_gates.shape[0]
    group_size = heads_dev // kv_dev
    score_scale = 1.0 / math.sqrt(HD)
    own_start = lax.axis_index("sp") * tok_rows
    own_last = own_start + tok_rows - 1
    first_doc = documents[0]
    query_pos = own_start + lax.iota(jnp.int32, tok_rows)
    query_heads = queries.reshape(tok_rows, kv_dev, group_size, HD)
    key_gates_all = log_gates.reshape(kv_dev, group_size, log_gates.shape[1])
    query_gates = lax.dynamic_slice_in_dim(key_gates_all, own_start, tok_rows, 2)
    collected = (
        lax.all_gather(gate_weight, "sp", axis=0, tiled=True),
        lax.all_gather(up_weight, "sp", axis=0, tiled=True),
        lax.all_gather(down_weight, "sp", axis=1, tiled=True),
    )
    residual_rows = resid.astype(jnp.float32)

    def attend_block(running, key_rows, value_rows, doc_rows, first_row):
        run_max, run_sum, accumulated = running
        key_count = key_rows.shape[0]
        scores = (
            jnp.einsum(
                "tkgd,skd->kgts",
                query_heads,
                key_rows.reshape(key_count, kv_dev, HD),
                preferred_element_type=jnp.float32,
            )
            * score_scale
        )
        key_gates = lax.dynamic_slice_in_dim(key_gates_all, first_row, key_count, 2)
        scores = scores + query_gates[..., None] - key_gates[:, :, None, :]
        key_pos = first_row + lax.iota(jnp.int32, key_count)
        visible = (key_pos[None, :] <= query_pos[:, None]) & (
            doc_rows[None, :] == documents[:, None]
        )
        scores = jnp.where(visible, scores, jnp.float32(-1e30))
        new_max = jnp.maximum(run_max, jnp.max(scores, axis=-1))
        probs = jnp.where(visible, jnp.exp(scores - new_max[..., None]), jnp.float32(0.0))
        shrink = jnp.exp(run_max - new_max)
        run_sum = run_sum * shrink + jnp.sum(probs, axis=-1)
        weighted = jnp.einsum(
            "kgts,skd->kgtd",
            probs.astype(jnp.bfloat16),
            value_rows.reshape(key_count, kv_dev, HD),
            preferred_element_type=jnp.float32,
        )
        accumulated = accumulated * shrink[..., None] + weighted
        return (new_max, run_sum, accumulated)

    def maybe_attend(running, key_rows, value_rows, doc_rows, first_row):
        needed = (first_row <= own_last) & (doc_rows[-1] >= first_doc)

        def compute(state):
            return attend_block(state, key_rows, value_rows, doc_rows, first_row)

        def keep(state):
            return state

        return lax.cond(needed, compute, keep, running)

    start_state = (
        jnp.full((kv_dev, group_size, tok_rows), -1e30, jnp.float32),
        jnp.zeros((kv_dev, group_size, tok_rows), jnp.float32),
        jnp.zeros((kv_dev, group_size, tok_rows, HD), jnp.float32),
    )
    key_rows = lax.all_gather(keys, "sp", axis=0, tiled=True)
    value_rows = lax.all_gather(values, "sp", axis=0, tiled=True)
    doc_rows = lax.all_gather(documents, "sp", axis=0, tiled=True)
    key_count = key_rows.shape[0]
    block_len = math.gcd(key_count, 1024)

    def advance(block_index, inner):
        offset = block_index * block_len
        return maybe_attend(
            inner,
            lax.dynamic_slice_in_dim(key_rows, offset, block_len, 0),
            lax.dynamic_slice_in_dim(value_rows, offset, block_len, 0),
            lax.dynamic_slice_in_dim(doc_rows, offset, block_len, 0),
            offset,
        )

    run_max, run_sum, accumulated = lax.fori_loop(0, key_count // block_len, advance, start_state)
    attended = accumulated / run_sum[..., None]
    attended = (
        jnp.transpose(attended, (2, 0, 1, 3)).reshape(tok_rows, heads_dev * HD).astype(jnp.bfloat16)
    )
    rows_slice = attended
    projected = lax.psum_scatter(
        jnp.dot(rows_slice, out_weight, preferred_element_type=jnp.float32).astype(jnp.bfloat16),
        "tp",
        scatter_dimension=0,
        tiled=True,
    ).astype(jnp.float32)
    power = jnp.mean(projected * projected, axis=-1, keepdims=True)
    middle = residual_rows + attn_gain * projected * lax.rsqrt(power + 1e-06)
    middle_power = jnp.mean(middle * middle, axis=-1, keepdims=True)
    normed = (mlp_gain * middle * lax.rsqrt(middle_power + 1e-06)).astype(jnp.bfloat16)
    normed_all = lax.all_gather(normed, "tp", axis=0, tiled=True)
    gate_full, up_full, down_full = collected
    gate_act = jnp.dot(normed_all, gate_full, preferred_element_type=jnp.float32)
    up_act = jnp.dot(normed_all, up_full, preferred_element_type=jnp.float32)
    hidden = (jax.nn.silu(gate_act) * up_act).astype(jnp.bfloat16)
    rows_slice = hidden
    lowered = lax.psum_scatter(
        jnp.dot(rows_slice, down_full, preferred_element_type=jnp.float32).astype(jnp.bfloat16),
        "tp",
        scatter_dimension=0,
        tiled=True,
    ).astype(jnp.float32)
    return (middle + 0.5 * lowered).astype(jnp.bfloat16)


GROUP = 4
PLANE = 4
MESH = pl.DeviceIdType.MESH
LOG2E = 1.4426950408889634
VMEM = pl.BlockSpec(memory_space=pltpu.VMEM)
K, V, DOC, GATE, UP, DOWN, Q = range(7)


def remote(src, dst, send_sem, recv_sem, target):
    return pltpu.make_async_remote_copy(
        src_ref=src,
        dst_ref=dst,
        send_sem=send_sem,
        recv_sem=recv_sem,
        device_id=target,
        device_id_type=MESH,
    )


def span(index, width):
    return pl.ds(pl.multiple_of(index * width, width), width)


def layer_kernel(
    q_ref, k_ref, v_ref, d_ref, lg_ref, ow_ref, resid_ref, ag_ref, mg_ref, g_ref, u_ref, w_ref,
    out_ref,
    kall, vall, docs, qs, gkc, gw, uw, dw, att, arr, pbuf, pgot, mid, nall, hid, part, pair, red,
    got,
    z_send, z_recv, p_send, p_recv, own_sem, a_send, a_recv, t_send, t_recv,
    o_send, n_send, n_recv, f_send, f_recv, x_send, x_recv, r_send, r_recv,
):
    me = lax.axis_index("sp")
    core = lax.axis_index("tp")
    z, p = me // PLANE, me % PLANE
    px, py = p % 2, p // 2
    other = 1 - core
    mate = (me, other)
    rows = k_ref.shape[0]
    qcols = q_ref.shape[1] // GROUP
    rank = qcols // HD
    fcols = g_ref.shape[1] // GROUP
    wrows, wcols = g_ref.shape[0], w_ref.shape[1]
    half, d_model = resid_ref.shape
    coef = LOG2E / math.sqrt(HD)
    neighbours = (1, 2, 3)

    def peer(e):
        x = px if e == 2 else 1 - px
        y = py if e == 1 else 1 - py
        return y * 2 + x

    def near(e):
        return (z * PLANE + peer(e), core)

    def there(zb):
        return (zb * PLANE + p, core)

    def place(a, k):
        if a == K:
            return kall.at[span(k, rows)]
        if a == V:
            return vall.at[span(k, rows)]
        if a == DOC:
            return docs.at[k]
        if a == GATE:
            return gw.at[span(k, wrows)]
        if a == UP:
            return uw.at[span(k, wrows)]
        if a == DOWN:
            return dw.at[:, span(k, wcols)]
        return qs.at[k // PLANE]

    def piece(a, to):
        if a == K:
            return k_ref.at[:, span(to, HD)]
        if a == V:
            return v_ref.at[:, span(to, HD)]
        if a == DOC:
            return d_ref.at[...]
        if a == GATE:
            return g_ref.at[:, span(to, fcols)]
        if a == UP:
            return u_ref.at[:, span(to, fcols)]
        if a == DOWN:
            return w_ref.at[span(to, fcols)]
        return q_ref.at[:, span(to, qcols)]

    barrier = pltpu.get_barrier_semaphore()
    for d in range(1, GROUP):
        pl.semaphore_signal(barrier, inc=1, device_id=there((z + d) % GROUP), device_id_type=MESH)
    for e in neighbours:
        pl.semaphore_signal(barrier, inc=1, device_id=near(e), device_id_type=MESH)
    pl.semaphore_signal(barrier, inc=1, device_id=mate, device_id_type=MESH)
    pl.semaphore_wait(barrier, 7)

    def z_copy(a, to):
        return remote(piece(a, to), place(a, me), z_send.at[a, to], z_recv.at[a, z], there(to))

    def z_sends(a):
        for d in (1, 3, 2):
            z_copy(a, (z + d) % GROUP).start()

    def z_arrival(a, zs):
        at = place(a, zs * PLANE + p)
        remote(at, at, z_send.at[a, z], z_recv.at[a, zs], mate).wait_recv()

    def own_copy(a):
        return pltpu.make_async_copy(piece(a, z), place(a, me), own_sem.at[a])

    def p_copy(a, zs, e):
        at = place(a, zs * PLANE + p)
        return remote(at, at, p_send.at[a, zs, e - 1], p_recv.at[a, zs, e - 1], near(e))

    def p_own(a, e):
        return remote(piece(a, z), place(a, me), p_send.at[a, z, e - 1], p_recv.at[a, z, e - 1],
                      near(e))

    def p_arrival(a, zs, e):
        at = place(a, zs * PLANE + peer(e))
        remote(at, at, p_send.at[a, zs, e - 1], p_recv.at[a, zs, e - 1], mate).wait_recv()

    def spread_own(a):
        for e in neighbours:
            p_own(a, e).start()

    def forward(a, zs):
        z_arrival(a, zs)
        for e in neighbours:
            p_copy(a, zs, e).start()

    for a in (DOC, K, V, Q, GATE):
        z_sends(a)
    for a in (DOC, K, V, GATE):
        spread_own(a)
    for a in range(7):
        own_copy(a).start()

    lanes = 128

    @pl.loop(0, kall.shape[0] // lanes)
    def _(j):
        at = span(j, lanes)
        for r in range(rank):
            row = lg_ref[z, r:r + 1, at] * LOG2E
            gkc[r, at, :] = jnp.transpose(jnp.broadcast_to(row, (lanes, lanes)))

    def ascending(i):
        return i + (i - z + GROUP) // GROUP

    @pl.loop(0, GROUP - 1)
    def _(i):
        forward(DOC, ascending(i))

    @pl.loop(0, GROUP - 1)
    def _(i):
        forward(K, ascending(i))
        forward(V, ascending(i))

    spread_own(UP)
    spread_own(DOWN)
    for a in range(7):
        own_copy(a).wait()
    for d in range(1, GROUP):
        z_arrival(Q, (z + d) % GROUP)

    @pl.loop(0, GROUP)
    def _(zs):
        for e in neighbours:
            p_arrival(DOC, zs, e)

    every_doc = docs[...]

    def below(level):
        total = jnp.sum((every_doc < level).astype(jnp.float32), axis=0)
        return jnp.sum(total, axis=1, keepdims=True)

    first_of_1, first_of_2 = below(1), below(2)

    @pl.loop(0, GROUP)
    def _(zq):
        for e in neighbours:
            p_arrival(K, zq, e)
            p_arrival(V, zq, e)
        block = zq * PLANE + p
        q = jnp.concatenate([qs[zq, :, r * HD:(r + 1) * HD] for r in range(rank)], axis=0)
        own = span(block, rows)
        gq = jnp.concatenate([lg_ref[z, r:r + 1, own] for r in range(rank)], axis=1) * LOG2E
        dq = docs[block]
        start = jnp.where(dq == 0, 0.0, jnp.where(dq == 1, first_of_1, first_of_2))
        start = jnp.concatenate([start.astype(jnp.int32)] * rank, axis=1)
        qpos = block * rows + lax.broadcasted_iota(jnp.int32, (1, rows), 1)
        qpos = jnp.concatenate([qpos] * rank, axis=1)

        def attend(base, count, causal, state):
            m, l, acc = state
            at = pl.ds(pl.multiple_of(base, count), count)
            s = lax.dot_general(kall[at], q, (((1,), (1,)), ((), ())),
                                preferred_element_type=jnp.float32)
            gk = jnp.concatenate(
                [gkc[r, at, :] for r in range(rank) for _ in range(rows // lanes)], axis=1)
            s = (s * coef + gq) - gk
            kpos = base + lax.broadcasted_iota(jnp.int32, (count, 1), 0)
            seen = kpos >= start
            if causal:
                seen = seen & (kpos <= qpos)
            s = jnp.where(seen, s, jnp.float32(-1e30))
            m_new = jnp.maximum(m, jnp.max(s, axis=0, keepdims=True))
            prob = jnp.exp2(s - m_new)
            shrink = jnp.exp2(m - m_new)
            l = l * shrink + jnp.sum(prob, axis=0, keepdims=True)
            acc = acc * shrink + lax.dot_general(
                vall[at], prob.astype(jnp.bfloat16), (((0,), (0,)), ((), ())),
                preferred_element_type=jnp.float32)
            return m_new, l, acc

        wide = 2 * rows
        state = (jnp.full((1, rank * rows), -1e20, jnp.float32),
                 jnp.zeros((1, rank * rows), jnp.float32),
                 jnp.zeros((HD, rank * rows), jnp.float32))
        state = lax.fori_loop(0, 2 * zq, lambda i, s: attend(i * wide, wide, False, s), state)
        m, l, acc = lax.fori_loop(
            0, p + 1, lambda i, s: attend((zq * PLANE + i) * rows, rows, True, s), state)
        res = acc / l
        for r in range(rank):
            att[zq, :, r * HD:(r + 1) * HD] = jnp.transpose(
                res[:, r * rows:(r + 1) * rows]).astype(jnp.bfloat16)

        @pl.when(zq != z)
        def _():
            remote(att.at[zq], arr.at[z], a_send.at[zq], a_recv.at[z], there(zq)).start()

        @pl.when(zq == 0)
        def _():
            z_sends(UP)

    own = pltpu.make_async_copy(att.at[z], arr.at[z], own_sem.at[0])
    own.start()
    own.wait()
    for d in range(1, GROUP):
        zs = (z + d) % GROUP
        at = arr.at[zs]
        remote(at, at, a_send.at[zs], a_recv.at[zs], mate).wait_recv()
    tile = 512

    @pl.loop(0, d_model // tile)
    def _(j):
        at = span(j, tile)
        total = jnp.dot(arr[0], ow_ref[0:qcols, at], preferred_element_type=jnp.float32)
        for g in range(1, GROUP):
            total += jnp.dot(arr[g], ow_ref[g * qcols:(g + 1) * qcols, at],
                             preferred_element_type=jnp.float32)
        pbuf[0, :, at] = total[:half].astype(jnp.bfloat16)
        pbuf[1, :, at] = total[half:].astype(jnp.bfloat16)

    swap = remote(pbuf.at[other], pgot, t_send, t_recv, mate)
    swap.start()
    swap.wait()
    projected = pbuf[core].astype(jnp.float32) + pgot[...].astype(jnp.float32)
    power = jnp.mean(projected * projected, axis=-1, keepdims=True)
    middle = resid_ref[...].astype(jnp.float32) + ag_ref[...] * projected * lax.rsqrt(power + 1e-06)
    mid[...] = middle
    mpower = jnp.mean(middle * middle, axis=-1, keepdims=True)
    nall[z, core] = (mg_ref[...] * middle * lax.rsqrt(mpower + 1e-06)).astype(jnp.bfloat16)

    def relay(zb, side, send_sem):
        block = nall.at[zb, core]
        return remote(block, block, send_sem, n_recv.at[zb],
                      ((z + 1 - 2 * side) * PLANE + p, core))

    def share(zb):
        block = nall.at[zb, core]
        return remote(block, block, f_send.at[zb], f_recv.at[zb], mate)

    def onward(side):
        return (side == 0) & (z < GROUP - 1) | (side == 1) & (z > 0)

    for side in (0, 1):
        @pl.when(onward(side))
        def _():
            relay(z, side, o_send.at[side]).start()
    share(z).start()
    z_sends(DOWN)

    def arrive(d):
        for side in (0, 1):
            zb = z - d if side == 0 else z + d

            @pl.when((zb >= 0) & (zb < GROUP))
            def _():
                block = nall.at[zb, core]
                remote(block, block, n_send.at[zb], n_recv.at[zb], mate).wait_recv()
                @pl.when(onward(side))
                def _():
                    relay(zb, side, n_send.at[zb]).start()
                share(zb).start()

    def forwards(a):
        for d in (1, 3, 2):
            forward(a, (z + d) % GROUP)

    forwards(GATE)
    forwards(UP)
    arrive(1)
    arrive(2)
    forwards(DOWN)
    arrive(3)

    @pl.loop(0, GROUP)
    def _(zs):
        for a in (GATE, UP):
            for e in neighbours:
                p_arrival(a, zs, e)

    @pl.loop(0, GROUP)
    def _(i):
        zb = (z + i) % GROUP
        over = nall.at[zb, other]
        remote(over, over, f_send.at[zb], f_recv.at[zb], mate).wait_recv()
        rows_in = jnp.concatenate([nall[zb, 0], nall[zb, 1]], axis=0)
        ftile = 256
        for j in range(fcols // ftile):
            at = slice(j * ftile, (j + 1) * ftile)
            gate = jnp.dot(rows_in, gw[:, at], preferred_element_type=jnp.float32)
            up = jnp.dot(rows_in, uw[:, at], preferred_element_type=jnp.float32)
            hid[zb, :, at] = (gate / (1.0 + jnp.exp(-gate)) * up).astype(jnp.bfloat16)

    gcols = PLANE * wcols

    def trade(zb, g):
        at = span(g, gcols)
        return remote(part.at[zb, other, :, at], pair.at[zb, :, at], x_send.at[zb, g],
                      x_recv.at[zb, g], mate)

    def give(zb, g):
        at = span(g, gcols)
        return remote(red.at[zb, :, at], got.at[z, :, at], r_send.at[zb, g], r_recv.at[z, g],
                      there(zb))

    def take(zb, g):
        at = span(g, gcols)
        remote(red.at[zb, :, at], got.at[zb, :, at], r_send.at[zb, g], r_recv.at[zb, g],
               mate).wait_recv()

    @pl.loop(0, GROUP)
    def _(i):
        g = (z + i) % GROUP
        at = span(g, gcols)
        for e in neighbours:
            p_arrival(DOWN, g, e)

        @pl.loop(1, GROUP + 1)
        def _(d):
            zb = (z + d) % GROUP
            total = jnp.dot(hid[zb], dw[:, at], preferred_element_type=jnp.float32)
            part[zb, 0, :, at] = total[:half].astype(jnp.bfloat16)
            part[zb, 1, :, at] = total[half:].astype(jnp.bfloat16)
            trade(zb, g).start()

        @pl.loop(1, GROUP)
        def _(d):
            zb = (z + d) % GROUP
            trade(zb, g).wait()
            red[zb, :, at] = (part[zb, core, :, at].astype(jnp.float32)
                              + pair[zb, :, at].astype(jnp.float32)).astype(jnp.bfloat16)
            give(zb, g).start()
        trade(z, g).wait()

    @pl.loop(0, GROUP)
    def _(i):
        g = (z + i) % GROUP
        for d in range(1, GROUP):
            take((z + d) % GROUP, (g + GROUP - d) % GROUP)

    @pl.loop(0, GROUP)
    def _(g):
        at = span(g, gcols)
        total = part[z, core, :, at].astype(jnp.float32) + pair[z, :, at].astype(jnp.float32)
        for d in range(1, GROUP):
            total += got[(z + d) % GROUP, :, at].astype(jnp.float32)
        out_ref[:, at] = (mid[:, at] + 0.5 * total).astype(jnp.bfloat16)

    for d in range(1, GROUP):
        zb = (z + d) % GROUP
        for a in range(7):
            z_copy(a, zb).wait_send()
        remote(att.at[zb], arr.at[z], a_send.at[zb], a_recv.at[z], there(zb)).wait_send()

        @pl.loop(0, GROUP)
        def _(g):
            give(zb, g).wait_send()
    for a in range(6):
        for e in neighbours:
            p_own(a, e).wait_send()
            for d in range(1, GROUP):
                p_copy(a, (z + d) % GROUP, e).wait_send()
    share(z).wait_send()
    for side in (0, 1):
        @pl.when(onward(side))
        def _():
            relay(z, side, o_send.at[side]).wait_send()
    for d in range(1, GROUP):
        share((z + d) % GROUP).wait_send()
        for side in (0, 1):
            zb = z - d if side == 0 else z + d

            @pl.when((zb >= 0) & (zb < GROUP) & onward(side))
            def _():
                relay(zb, side, n_send.at[zb]).wait_send()


def grouped(
    sp, resid, queries, keys, values, log_gates, documents, out_weight, attn_gain, mlp_gain,
    gate_weight, up_weight, down_weight,
):
    rows, ff = keys.shape[0], gate_weight.shape[1] // GROUP
    half, d_model = resid.shape
    tokens = rows * sp
    qcols = queries.shape[1] // GROUP
    rank = qcols // HD
    bf, f32 = jnp.bfloat16, jnp.float32
    dma = pltpu.SemaphoreType.DMA
    return pl.pallas_call(
        layer_kernel,
        out_shape=jax.ShapeDtypeStruct(resid.shape, bf),
        in_specs=[VMEM] * 12,
        out_specs=VMEM,
        scratch_shapes=[
            pltpu.VMEM((tokens, HD), bf),
            pltpu.VMEM((tokens, HD), bf),
            pltpu.VMEM((sp, 1, rows), jnp.int32),
            pltpu.VMEM((GROUP, rows, qcols), bf),
            pltpu.VMEM((rank, tokens, 128), f32),
            pltpu.VMEM((d_model, ff), bf),
            pltpu.VMEM((d_model, ff), bf),
            pltpu.VMEM((ff, d_model), bf),
            pltpu.VMEM((GROUP, rows, qcols), bf),
            pltpu.VMEM((GROUP, rows, qcols), bf),
            pltpu.VMEM((2, half, d_model), bf),
            pltpu.VMEM((half, d_model), bf),
            pltpu.VMEM((half, d_model), f32),
            pltpu.VMEM((GROUP, 2, half, d_model), bf),
            pltpu.VMEM((GROUP, rows, ff), bf),
            pltpu.VMEM((GROUP, 2, half, d_model), bf),
            pltpu.VMEM((GROUP, half, d_model), bf),
            pltpu.VMEM((GROUP, half, d_model), bf),
            pltpu.VMEM((GROUP, half, d_model), bf),
            dma((7, GROUP)), dma((7, GROUP)), dma((6, GROUP, 3)), dma((6, GROUP, 3)), dma((7,)),
            dma((GROUP,)), dma((GROUP,)), dma, dma,
            dma((2,)), dma((GROUP,)), dma((GROUP,)), dma((GROUP,)), dma((GROUP,)),
            dma((GROUP, GROUP)), dma((GROUP, GROUP)), dma((GROUP, GROUP)), dma((GROUP, GROUP)),
        ],
        compiler_params=pltpu.CompilerParams(
            collective_id=0, has_side_effects=True, vmem_limit_bytes=62 * 1024 * 1024),
    )(queries, keys, values, documents[None, :], log_gates.reshape(GROUP, rank, tokens),
      out_weight, resid, attn_gain[None, :], mlp_gain[None, :], gate_weight, up_weight,
      down_weight)


def solution(mesh):
    placed = (
        P(("sp", "tp"), None),
        P("sp", "tp"),
        P("sp", "tp"),
        P("sp", "tp"),
        P("tp", None),
        P("sp"),
        P("tp", None),
        P(),
        P(),
        P("sp", "tp"),
        P("sp", "tp"),
        P("tp", "sp"),
    )
    sp, tp = mesh.shape["sp"], mesh.shape["tp"]

    def layer(*args):
        kv_dev = args[2].shape[1] // HD
        fits = tp == 2 and sp == GROUP * PLANE and kv_dev == GROUP
        return grouped(sp, *args) if fits else local(*args)

    return jax.shard_map(
        layer, mesh=mesh, in_specs=placed, out_specs=P(("sp", "tp"), None), check_vma=False
    )
```

time: 203 us -> 171 us (0.84)
  the two profiles are of different devices: /device:TPU:10 before, /device:TPU:0 now
where the time goes in v1:
time: 171 us; the launch traced here: 169 us
  Pallas kernels  165 us (96%)
  local copies, waits for them, and re-layouts  3.52 us (2%)
    pallas_call x1, Pallas kernels, grouped(): pl.pallas_call(layer_kernel, out_shape=jax.ShapeDtypeStruct(resid.shape,...  165 us

profile of v1, /device:TPU:0, one launch (start us, length us, event | category | flops | bytes accessed | tf_op | source)
XLA Modules:
  0.0 168.7 jit_solution(14047588817909529376)
XLA Ops:
  0.0 1.6 reshape.3.lg_ref
  1.6 165.1 %shard_map.118 = bf16[128,2048]{1,0:T(8,128)(2,1)} custom-call(bf16[256,1024]{1,0:T(8,128)(2,1)} %q_ref.1, bf16[256,512]{1,0:T(8,128)(2,1)} %k_ref.1, bf16[256,512]{1,0:T(8,128)(2,1)} %v_ref.1, s32[1,256]{1,0:T(1,128)} %bitcast.5, f32[4,2,4096]{2,1,0:T(2,128)} %reshape.3.lg_ref, bf16[1024,2048]{1,0:T(8,128)(2,1)} %ow_ref.1, bf16[128,2048]{1,0:T(8,128)(2,1)} %resid_ref.1, ...), custom_call_target="tpu_custom_call" | custom-call | tf_op jit(solution)/shard_map/pallas_call | solution.py:562
  166.8 1.9 %copy.14 = bf16[128,2048]{1,0:T(8,128)(2,1)} copy(bf16[128,2048]{1,0:T(8,128)(2,1)} %shard_map.118) | data formatting | bytes 1048576

commit v2 on v1

--- a/solution.py
+++ b/solution.py
@@ -143,6 +143,7 @@
 MESH = pl.DeviceIdType.MESH
 LOG2E = 1.4426950408889634
 VMEM = pl.BlockSpec(memory_space=pltpu.VMEM)
+ANY = pl.BlockSpec(memory_space=pl.ANY)
 K, V, DOC, GATE, UP, DOWN, Q = range(7)
 
 
@@ -162,12 +163,13 @@
 
 
 def layer_kernel(
-    q_ref, k_ref, v_ref, d_ref, lg_ref, ow_ref, resid_ref, ag_ref, mg_ref, g_ref, u_ref, w_ref,
+    q_ref, k_ref, v_ref, d_ref, lg_ref, ow_hbm, resid_hbm, ag_ref, mg_ref, g_ref, u_ref, w_ref,
     out_ref,
+    ow_ref, resid_ref,
     kall, vall, docs, qs, gkc, gw, uw, dw, att, arr, pbuf, pgot, mid, nall, hid, part, pair, red,
-    got,
-    z_send, z_recv, p_send, p_recv, own_sem, a_send, a_recv, t_send, t_recv,
-    o_send, n_send, n_recv, f_send, f_recv, x_send, x_recv, r_send, r_recv,
+    got, comb,
+    z_send, z_recv, p_send, p_recv, own_sem, load_sem, a_send, a_recv, t_send, t_recv,
+    o_send, n_send, n_recv, f_send, f_recv, x_send, x_recv, r_send, r_recv, c_recv,
 ):
     me = lax.axis_index("sp")
     core = lax.axis_index("tp")
@@ -180,7 +182,7 @@
     rank = qcols // HD
     fcols = g_ref.shape[1] // GROUP
     wrows, wcols = g_ref.shape[0], w_ref.shape[1]
-    half, d_model = resid_ref.shape
+    half, d_model = resid_hbm.shape
     coef = LOG2E / math.sqrt(HD)
     neighbours = (1, 2, 3)
 
@@ -228,6 +230,8 @@
     barrier = pltpu.get_barrier_semaphore()
     for d in range(1, GROUP):
         pl.semaphore_signal(barrier, inc=1, device_id=there((z + d) % GROUP), device_id_type=MESH)
+    loads = (pltpu.make_async_copy(ow_hbm, ow_ref, load_sem.at[0]),
+             pltpu.make_async_copy(resid_hbm, resid_ref, load_sem.at[1]))
     for e in neighbours:
         pl.semaphore_signal(barrier, inc=1, device_id=near(e), device_id_type=MESH)
     pl.semaphore_signal(barrier, inc=1, device_id=mate, device_id_type=MESH)
@@ -270,18 +274,25 @@
 
     for a in (DOC, K, V, Q, GATE):
         z_sends(a)
-    for a in (DOC, K, V, GATE):
+    for a in (DOC, K, V):
         spread_own(a)
     for a in range(7):
         own_copy(a).start()
+    for load in loads:
+        load.start()
 
     lanes = 128
+
+    def gate_row(r, at):
+        block = lg_ref[:, at]
+        chosen = lax.broadcasted_iota(jnp.int32, block.shape, 0) == z * rank + r
+        return jnp.sum(jnp.where(chosen, block, 0.0), axis=0, keepdims=True) * LOG2E
 
     @pl.loop(0, kall.shape[0] // lanes)
     def _(j):
         at = span(j, lanes)
         for r in range(rank):
-            row = lg_ref[z, r:r + 1, at] * LOG2E
+            row = gate_row(r, at)
             gkc[r, at, :] = jnp.transpose(jnp.broadcast_to(row, (lanes, lanes)))
 
     def ascending(i):
@@ -291,17 +302,13 @@
     def _(i):
         forward(DOC, ascending(i))
 
-    @pl.loop(0, GROUP - 1)
+    @pl.loop(0, GROUP - 2)
     def _(i):
         forward(K, ascending(i))
         forward(V, ascending(i))
 
-    spread_own(UP)
-    spread_own(DOWN)
     for a in range(7):
         own_copy(a).wait()
-    for d in range(1, GROUP):
-        z_arrival(Q, (z + d) % GROUP)
 
     @pl.loop(0, GROUP)
     def _(zs):
@@ -318,13 +325,24 @@
 
     @pl.loop(0, GROUP)
     def _(zq):
+        @pl.when(zq == 1)
+        def _():
+            forward(K, ascending(GROUP - 2))
+            forward(V, ascending(GROUP - 2))
+            spread_own(GATE)
+            spread_own(UP)
+
+        @pl.when(zq != z)
+        def _():
+            z_arrival(Q, zq)
+
         for e in neighbours:
             p_arrival(K, zq, e)
             p_arrival(V, zq, e)
         block = zq * PLANE + p
         q = jnp.concatenate([qs[zq, :, r * HD:(r + 1) * HD] for r in range(rank)], axis=0)
         own = span(block, rows)
-        gq = jnp.concatenate([lg_ref[z, r:r + 1, own] for r in range(rank)], axis=1) * LOG2E
+        gq = jnp.concatenate([gate_row(r, own) for r in range(rank)], axis=1)
         dq = docs[block]
         start = jnp.where(dq == 0, 0.0, jnp.where(dq == 1, first_of_1, first_of_2))
         start = jnp.concatenate([start.astype(jnp.int32)] * rank, axis=1)
@@ -369,10 +387,16 @@
         def _():
             remote(att.at[zq], arr.at[z], a_send.at[zq], a_recv.at[z], there(zq)).start()
 
-        @pl.when(zq == 0)
-        def _():
-            z_sends(UP)
-
+    def forwards(a):
+        @pl.loop(0, GROUP - 1)
+        def _(i):
+            forward(a, ascending(i))
+
+    z_sends(UP)
+    forwards(GATE)
+    spread_own(DOWN)
+    for load in loads:
+        load.wait()
     own = pltpu.make_async_copy(att.at[z], arr.at[z], own_sem.at[0])
     own.start()
     own.wait()
@@ -419,7 +443,6 @@
         def _():
             relay(z, side, o_send.at[side]).start()
     share(z).start()
-    z_sends(DOWN)
 
     def arrive(d):
         for side in (0, 1):
@@ -434,26 +457,11 @@
                     relay(zb, side, n_send.at[zb]).start()
                 share(zb).start()
 
-    def forwards(a):
-        for d in (1, 3, 2):
-            forward(a, (z + d) % GROUP)
-
-    forwards(GATE)
-    forwards(UP)
-    arrive(1)
-    arrive(2)
-    forwards(DOWN)
-    arrive(3)
-
-    @pl.loop(0, GROUP)
-    def _(zs):
-        for a in (GATE, UP):
-            for e in neighbours:
-                p_arrival(a, zs, e)
-
-    @pl.loop(0, GROUP)
-    def _(i):
-        zb = (z + i) % GROUP
+    mate_z = z + 1 - 2 * (z % 2)
+    far = GROUP // 2 - (z // 2) * 2
+    at_end = (z == 0) | (z == GROUP - 1)
+
+    def expand(zb):
         over = nall.at[zb, other]
         remote(over, over, f_send.at[zb], f_recv.at[zb], mate).wait_recv()
         rows_in = jnp.concatenate([nall[zb, 0], nall[zb, 1]], axis=0)
@@ -471,52 +479,94 @@
         return remote(part.at[zb, other, :, at], pair.at[zb, :, at], x_send.at[zb, g],
                       x_recv.at[zb, g], mate)
 
+    def lower(zb, g):
+        at = span(g, gcols)
+        total = jnp.dot(hid[zb], dw[:, at], preferred_element_type=jnp.float32)
+        part[zb, 0, :, at] = total[:half].astype(jnp.bfloat16)
+        part[zb, 1, :, at] = total[half:].astype(jnp.bfloat16)
+        trade(zb, g).start()
+
+    def both(zb, at):
+        return part[zb, core, :, at].astype(jnp.float32) + pair[zb, :, at].astype(jnp.float32)
+
     def give(zb, g):
         at = span(g, gcols)
-        return remote(red.at[zb, :, at], got.at[z, :, at], r_send.at[zb, g], r_recv.at[z, g],
+        return remote(red.at[zb, :, at], got.at[0, :, at], r_send.at[zb, g], r_recv.at[0, g],
                       there(zb))
 
-    def take(zb, g):
+    def give_far(zb, g):
         at = span(g, gcols)
-        remote(red.at[zb, :, at], got.at[zb, :, at], r_send.at[zb, g], r_recv.at[zb, g],
-               mate).wait_recv()
+        return remote(red.at[zb, :, at], got.at[1, :, at], r_send.at[zb, g], r_recv.at[1, g],
+                      there(zb))
+
+    def give_comb(j, g):
+        at = span(g, gcols)
+        return remote(red.at[far + j, :, at], comb.at[j, :, at], r_send.at[far + j, g],
+                      c_recv.at[j, g], there(mate_z))
+
+    forwards(UP)
+    arrive(1)
+    z_sends(DOWN)
+    arrive(2)
 
     @pl.loop(0, GROUP)
-    def _(i):
-        g = (z + i) % GROUP
+    def _(zs):
+        for a in (GATE, UP):
+            for e in neighbours:
+                p_arrival(a, zs, e)
+
+    expand(z)
+    expand(mate_z)
+    forwards(DOWN)
+    arrive(3)
+
+    @pl.loop(0, GROUP)
+    def _(g):
         at = span(g, gcols)
         for e in neighbours:
             p_arrival(DOWN, g, e)
-
-        @pl.loop(1, GROUP + 1)
-        def _(d):
-            zb = (z + d) % GROUP
-            total = jnp.dot(hid[zb], dw[:, at], preferred_element_type=jnp.float32)
-            part[zb, 0, :, at] = total[:half].astype(jnp.bfloat16)
-            part[zb, 1, :, at] = total[half:].astype(jnp.bfloat16)
-            trade(zb, g).start()
-
-        @pl.loop(1, GROUP)
-        def _(d):
-            zb = (z + d) % GROUP
-            trade(zb, g).wait()
-            red[zb, :, at] = (part[zb, core, :, at].astype(jnp.float32)
-                              + pair[zb, :, at].astype(jnp.float32)).astype(jnp.bfloat16)
-            give(zb, g).start()
+        lower(mate_z, g)
+        lower(z, g)
+        trade(mate_z, g).wait()
+        red[mate_z, :, at] = both(mate_z, at).astype(jnp.bfloat16)
+        give(mate_z, g).start()
         trade(z, g).wait()
 
-    @pl.loop(0, GROUP)
-    def _(i):
-        g = (z + i) % GROUP
-        for d in range(1, GROUP):
-            take((z + d) % GROUP, (g + GROUP - d) % GROUP)
+    @pl.loop(0, 2)
+    def _(j):
+        expand(far + j)
+
+    @pl.loop(0, GROUP + 1)
+    def _(s):
+        @pl.when(s < GROUP)
+        def _():
+            at = span(s, gcols)
+            for j in (0, 1):
+                lower(far + j, s)
+            for j in (0, 1):
+                trade(far + j, s).wait()
+
+                @pl.when(at_end)
+                def _():
+                    red[far + j, :, at] = both(far + j, at).astype(jnp.bfloat16)
+                    give_comb(j, s).start()
+
+        @pl.when((s > 0) & (z > 0) & (z < GROUP - 1))
+        def _():
+            g = s - 1
+            at = span(g, gcols)
+            for j in (0, 1):
+                give_comb(j, g).wait_recv()
+                red[far + j, :, at] = (both(far + j, at)
+                                       + comb[j, :, at].astype(jnp.float32)).astype(jnp.bfloat16)
+                give_far(far + j, g).start()
 
     @pl.loop(0, GROUP)
     def _(g):
         at = span(g, gcols)
-        total = part[z, core, :, at].astype(jnp.float32) + pair[z, :, at].astype(jnp.float32)
-        for d in range(1, GROUP):
-            total += got[(z + d) % GROUP, :, at].astype(jnp.float32)
+        give(mate_z, g).wait_recv()
+        give_far(far, g).wait_recv()
+        total = both(z, at) + got[0, :, at].astype(jnp.float32) + got[1, :, at].astype(jnp.float32)
         out_ref[:, at] = (mid[:, at] + 0.5 * total).astype(jnp.bfloat16)
 
     for d in range(1, GROUP):
@@ -528,6 +578,7 @@
         @pl.loop(0, GROUP)
         def _(g):
             give(zb, g).wait_send()
+
     for a in range(6):
         for e in neighbours:
             p_own(a, e).wait_send()
@@ -562,9 +613,11 @@
     return pl.pallas_call(
         layer_kernel,
         out_shape=jax.ShapeDtypeStruct(resid.shape, bf),
-        in_specs=[VMEM] * 12,
+        in_specs=[VMEM] * 5 + [ANY] * 2 + [VMEM] * 2 + [ANY] * 3,
         out_specs=VMEM,
         scratch_shapes=[
+            pltpu.VMEM(out_weight.shape, bf),
+            pltpu.VMEM(resid.shape, bf),
             pltpu.VMEM((tokens, HD), bf),
             pltpu.VMEM((tokens, HD), bf),
             pltpu.VMEM((sp, 1, rows), jnp.int32),
@@ -583,15 +636,18 @@
             pltpu.VMEM((GROUP, 2, half, d_model), bf),
             pltpu.VMEM((GROUP, half, d_model), bf),
             pltpu.VMEM((GROUP, half, d_model), bf),
-            pltpu.VMEM((GROUP, half, d_model), bf),
+            pltpu.VMEM((2, half, d_model), bf),
+            pltpu.VMEM((2, half, d_model), bf),
             dma((7, GROUP)), dma((7, GROUP)), dma((6, GROUP, 3)), dma((6, GROUP, 3)), dma((7,)),
+            dma((2,)),
             dma((GROUP,)), dma((GROUP,)), dma, dma,
             dma((2,)), dma((GROUP,)), dma((GROUP,)), dma((GROUP,)), dma((GROUP,)),
-            dma((GROUP, GROUP)), dma((GROUP, GROUP)), dma((GROUP, GROUP)), dma((GROUP, GROUP)),
+            dma((GROUP, GROUP)), dma((GROUP, GROUP)), dma((GROUP, GROUP)), dma((2, GROUP)),
+            dma((2, GROUP)),
         ],
         compiler_params=pltpu.CompilerParams(
             collective_id=0, has_side_effects=True, vmem_limit_bytes=62 * 1024 * 1024),
-    )(queries, keys, values, documents[None, :], log_gates.reshape(GROUP, rank, tokens),
+    )(queries, keys, values, documents[None, :], log_gates,
       out_weight, resid, attn_gain[None, :], mlp_gain[None, :], gate_weight, up_weight,
       down_weight)
 

time: 171 us -> 157 us (0.918)
  Pallas kernels: 165 us -> 153 us
    pallas_call x1, Pallas kernels: 165 us -> 153 us  [grouped(): pl.pallas_call(layer_kernel, out_shape=jax.ShapeDtypeStruct(resid.shape,...]
where the time goes in v2:
time: 157 us; the launch traced here: 155 us
  Pallas kernels  153 us (97%)
  local copies, waits for them, and re-layouts  1.88 us (1%)
    pallas_call x1, Pallas kernels, grouped(): pl.pallas_call(layer_kernel, out_shape=jax.ShapeDtypeStruct(resid.shape,...  153 us

profile of v2, /device:TPU:0, one launch (start us, length us, event | category | flops | bytes accessed | tf_op | source)
XLA Modules:
  0.0 155.1 jit_solution(3277471289240710578)
XLA Ops:
  0.0 153.2 %shard_map.118 = bf16[128,2048]{1,0:T(8,128)(2,1)} custom-call(bf16[256,1024]{1,0:T(8,128)(2,1)} %q_ref.1, bf16[256,512]{1,0:T(8,128)(2,1)} %k_ref.1, bf16[256,512]{1,0:T(8,128)(2,1)} %v_ref.1, s32[1,256]{1,0:T(1,128)} %bitcast.5, f32[8,4096]{1,0:T(8,128)} %lg_ref.1, bf16[1024,2048]{1,0:T(8,128)(2,1)} %ow_hbm.1, bf16[128,2048]{1,0:T(8,128)(2,1)} %resid_hbm.1, ...), custom_call_target="tpu_custom_call" | custom-call | tf_op jit(solution)/shard_map/pallas_call | solution.py:613
  153.2 1.9 %copy.14 = bf16[128,2048]{1,0:T(8,128)(2,1)} copy(bf16[128,2048]{1,0:T(8,128)(2,1)} %shard_map.118) | data formatting | bytes 1048576

commit v3 on v2

--- a/solution.py
+++ b/solution.py
@@ -298,9 +298,12 @@
     def ascending(i):
         return i + (i - z + GROUP) // GROUP
 
-    @pl.loop(0, GROUP - 1)
-    def _(i):
-        forward(DOC, ascending(i))
+    def forwards(a):
+        @pl.loop(0, GROUP - 1)
+        def _(i):
+            forward(a, ascending(i))
+
+    forwards(DOC)
 
     @pl.loop(0, GROUP - 2)
     def _(i):
@@ -331,6 +334,11 @@
             forward(V, ascending(GROUP - 2))
             spread_own(GATE)
             spread_own(UP)
+            z_sends(UP)
+
+        @pl.when(zq == GROUP - 1)
+        def _():
+            forwards(GATE)
 
         @pl.when(zq != z)
         def _():
@@ -387,13 +395,8 @@
         def _():
             remote(att.at[zq], arr.at[z], a_send.at[zq], a_recv.at[z], there(zq)).start()
 
-    def forwards(a):
-        @pl.loop(0, GROUP - 1)
-        def _(i):
-            forward(a, ascending(i))
-
-    z_sends(UP)
-    forwards(GATE)
+    z_sends(DOWN)
+    forwards(UP)
     spread_own(DOWN)
     for load in loads:
         load.wait()
@@ -426,53 +429,62 @@
     mpower = jnp.mean(middle * middle, axis=-1, keepdims=True)
     nall[z, core] = (mg_ref[...] * middle * lax.rsqrt(mpower + 1e-06)).astype(jnp.bfloat16)
 
-    def relay(zb, side, send_sem):
-        block = nall.at[zb, core]
-        return remote(block, block, send_sem, n_recv.at[zb],
+    piece_rows = half // 2
+
+    def relay(zb, side, c, send_sem):
+        block = nall.at[zb, core, span(c, piece_rows)]
+        return remote(block, block, send_sem, n_recv.at[zb, c],
                       ((z + 1 - 2 * side) * PLANE + p, core))
 
-    def share(zb):
-        block = nall.at[zb, core]
-        return remote(block, block, f_send.at[zb], f_recv.at[zb], mate)
+    def share(zb, c):
+        block = nall.at[zb, core, span(c, piece_rows)]
+        return remote(block, block, f_send.at[zb, c], f_recv.at[zb, c], mate)
+
+    def shared(zb, c):
+        over = nall.at[zb, other, span(c, piece_rows)]
+        remote(over, over, f_send.at[zb, c], f_recv.at[zb, c], mate).wait_recv()
 
     def onward(side):
         return (side == 0) & (z < GROUP - 1) | (side == 1) & (z > 0)
 
-    for side in (0, 1):
-        @pl.when(onward(side))
-        def _():
-            relay(z, side, o_send.at[side]).start()
-    share(z).start()
-
-    def arrive(d):
+    for c in (0, 1):
+        for side in (0, 1):
+            @pl.when(onward(side))
+            def _():
+                relay(z, side, c, o_send.at[side, c]).start()
+    for c in (0, 1):
+        share(z, c).start()
+
+    def arrive(d, c):
         for side in (0, 1):
             zb = z - d if side == 0 else z + d
 
             @pl.when((zb >= 0) & (zb < GROUP))
             def _():
-                block = nall.at[zb, core]
-                remote(block, block, n_send.at[zb], n_recv.at[zb], mate).wait_recv()
+                block = nall.at[zb, core, span(c, piece_rows)]
+                remote(block, block, n_send.at[zb, c], n_recv.at[zb, c], mate).wait_recv()
                 @pl.when(onward(side))
                 def _():
-                    relay(zb, side, n_send.at[zb]).start()
-                share(zb).start()
+                    relay(zb, side, c, n_send.at[zb, c]).start()
+                share(zb, c).start()
 
     mate_z = z + 1 - 2 * (z % 2)
     far = GROUP // 2 - (z // 2) * 2
     at_end = (z == 0) | (z == GROUP - 1)
 
-    def expand(zb):
-        over = nall.at[zb, other]
-        remote(over, over, f_send.at[zb], f_recv.at[zb], mate).wait_recv()
-        rows_in = jnp.concatenate([nall[zb, 0], nall[zb, 1]], axis=0)
+    def expand(zb, c):
+        shared(zb, c)
+        rows_in = jnp.concatenate(
+            [nall[zb, i, span(c, piece_rows), :] for i in (0, 1)], axis=0)
         ftile = 256
         for j in range(fcols // ftile):
             at = slice(j * ftile, (j + 1) * ftile)
             gate = jnp.dot(rows_in, gw[:, at], preferred_element_type=jnp.float32)
             up = jnp.dot(rows_in, uw[:, at], preferred_element_type=jnp.float32)
-            hid[zb, :, at] = (gate / (1.0 + jnp.exp(-gate)) * up).astype(jnp.bfloat16)
+            hid[zb, c, :, at] = (gate / (1.0 + jnp.exp(-gate)) * up).astype(jnp.bfloat16)
 
     gcols = PLANE * wcols
+    hcols = d_model // 2
 
     def trade(zb, g):
         at = span(g, gcols)
@@ -481,9 +493,13 @@
 
     def lower(zb, g):
         at = span(g, gcols)
-        total = jnp.dot(hid[zb], dw[:, at], preferred_element_type=jnp.float32)
-        part[zb, 0, :, at] = total[:half].astype(jnp.bfloat16)
-        part[zb, 1, :, at] = total[half:].astype(jnp.bfloat16)
+        rows_in = jnp.concatenate([hid[zb, 0], hid[zb, 1]], axis=0)
+        total = jnp.dot(rows_in, dw[:, at], preferred_element_type=jnp.float32)
+        for c in (0, 1):
+            for i in (0, 1):
+                first = (2 * c + i) * piece_rows
+                part[zb, i, c * piece_rows:(c + 1) * piece_rows, at] = (
+                    total[first:first + piece_rows].astype(jnp.bfloat16))
         trade(zb, g).start()
 
     def both(zb, at):
@@ -494,20 +510,30 @@
         return remote(red.at[zb, :, at], got.at[0, :, at], r_send.at[zb, g], r_recv.at[0, g],
                       there(zb))
 
-    def give_far(zb, g):
-        at = span(g, gcols)
-        return remote(red.at[zb, :, at], got.at[1, :, at], r_send.at[zb, g], r_recv.at[1, g],
-                      there(zb))
-
-    def give_comb(j, g):
-        at = span(g, gcols)
-        return remote(red.at[far + j, :, at], comb.at[j, :, at], r_send.at[far + j, g],
-                      c_recv.at[j, g], there(mate_z))
-
-    forwards(UP)
-    arrive(1)
-    z_sends(DOWN)
-    arrive(2)
+    def corner(c, h):
+        return span(c, piece_rows), slice(h * hcols, (h + 1) * hcols)
+
+    def trade_far(zb, c, h):
+        rs, cs = corner(c, h)
+        return remote(part.at[zb, other, rs, cs], pair.at[zb, rs, cs], x_send.at[zb, 2 * c + h],
+                      x_recv.at[zb, 2 * c + h], mate)
+
+    def give_far(zb, c, h):
+        rs, cs = corner(c, h)
+        return remote(red.at[zb, rs, cs], got.at[1, rs, cs], r_send.at[zb, 2 * c + h],
+                      r_recv.at[1, 2 * c + h], there(zb))
+
+    def give_comb(t, zb, c, h):
+        rs, cs = corner(c, h)
+        return remote(red.at[zb, rs, cs], comb.at[t, rs, cs], r_send.at[zb, 2 * c + h],
+                      c_recv.at[t, 2 * c + h], there(mate_z))
+
+    def both_far(zb, rs, cs):
+        return part[zb, core, rs, cs].astype(jnp.float32) + pair[zb, rs, cs].astype(jnp.float32)
+
+    forwards(DOWN)
+    arrive(1, 0)
+    arrive(1, 1)
 
     @pl.loop(0, GROUP)
     def _(zs):
@@ -515,10 +541,14 @@
             for e in neighbours:
                 p_arrival(a, zs, e)
 
-    expand(z)
-    expand(mate_z)
-    forwards(DOWN)
-    arrive(3)
+    @pl.loop(0, 2)
+    def _(c):
+        expand(z, c)
+        arrive(2, c)
+
+    @pl.loop(0, 2)
+    def _(c):
+        expand(mate_z, c)
 
     @pl.loop(0, GROUP)
     def _(g):
@@ -532,40 +562,52 @@
         give(mate_z, g).start()
         trade(z, g).wait()
 
-    @pl.loop(0, 2)
-    def _(j):
-        expand(far + j)
-
-    @pl.loop(0, GROUP + 1)
-    def _(s):
-        @pl.when(s < GROUP)
-        def _():
-            at = span(s, gcols)
-            for j in (0, 1):
-                lower(far + j, s)
-            for j in (0, 1):
-                trade(far + j, s).wait()
+    def send_far(t):
+        zb = far + t + (1 - 2 * t) * (z // 2)
+
+        @pl.loop(0, 2)
+        def _(c):
+            if t == 1:
+                arrive(3, c)
+            expand(zb, c)
+            for h in (0, 1):
+                rs, cs = corner(c, h)
+                total = jnp.dot(hid[zb, c], dw[:, cs], preferred_element_type=jnp.float32)
+                for i in (0, 1):
+                    part[zb, i, rs, cs] = total[i * piece_rows:(i + 1) * piece_rows].astype(
+                        jnp.bfloat16)
+                trade_far(zb, c, h).start()
+            for h in (0, 1):
+                rs, cs = corner(c, h)
+                trade_far(zb, c, h).wait()
 
                 @pl.when(at_end)
                 def _():
-                    red[far + j, :, at] = both(far + j, at).astype(jnp.bfloat16)
-                    give_comb(j, s).start()
-
-        @pl.when((s > 0) & (z > 0) & (z < GROUP - 1))
+                    red[zb, rs, cs] = both_far(zb, rs, cs).astype(jnp.bfloat16)
+                    give_comb(t, zb, c, h).start()
+
+        @pl.when((z > 0) & (z < GROUP - 1))
         def _():
-            g = s - 1
-            at = span(g, gcols)
-            for j in (0, 1):
-                give_comb(j, g).wait_recv()
-                red[far + j, :, at] = (both(far + j, at)
-                                       + comb[j, :, at].astype(jnp.float32)).astype(jnp.bfloat16)
-                give_far(far + j, g).start()
+            @pl.loop(0, 2)
+            def _(c):
+                for h in (0, 1):
+                    rs, cs = corner(c, h)
+                    give_comb(t, zb, c, h).wait_recv()
+                    red[zb, rs, cs] = (both_far(zb, rs, cs)
+                                       + comb[t, rs, cs].astype(jnp.float32)).astype(jnp.bfloat16)
+                    give_far(zb, c, h).start()
+
+    send_far(0)
+    send_far(1)
+
+    for c in (0, 1):
+        for h in (0, 1):
+            give_far(far, c, h).wait_recv()
 
     @pl.loop(0, GROUP)
     def _(g):
         at = span(g, gcols)
         give(mate_z, g).wait_recv()
-        give_far(far, g).wait_recv()
         total = both(z, at) + got[0, :, at].astype(jnp.float32) + got[1, :, at].astype(jnp.float32)
         out_ref[:, at] = (mid[:, at] + 0.5 * total).astype(jnp.bfloat16)
 
@@ -584,19 +626,20 @@
             p_own(a, e).wait_send()
             for d in range(1, GROUP):
                 p_copy(a, (z + d) % GROUP, e).wait_send()
-    share(z).wait_send()
-    for side in (0, 1):
-        @pl.when(onward(side))
-        def _():
-            relay(z, side, o_send.at[side]).wait_send()
-    for d in range(1, GROUP):
-        share((z + d) % GROUP).wait_send()
+    for c in (0, 1):
+        share(z, c).wait_send()
         for side in (0, 1):
-            zb = z - d if side == 0 else z + d
-
-            @pl.when((zb >= 0) & (zb < GROUP) & onward(side))
+            @pl.when(onward(side))
             def _():
-                relay(zb, side, n_send.at[zb]).wait_send()
+                relay(z, side, c, o_send.at[side, c]).wait_send()
+        for d in range(1, GROUP):
+            share((z + d) % GROUP, c).wait_send()
+            for side in (0, 1):
+                zb = z - d if side == 0 else z + d
+
+                @pl.when((zb >= 0) & (zb < GROUP) & onward(side))
+                def _():
+                    relay(zb, side, c, n_send.at[zb, c]).wait_send()
 
 
 def grouped(
@@ -632,7 +675,7 @@
             pltpu.VMEM((half, d_model), bf),
             pltpu.VMEM((half, d_model), f32),
             pltpu.VMEM((GROUP, 2, half, d_model), bf),
-            pltpu.VMEM((GROUP, rows, ff), bf),
+            pltpu.VMEM((GROUP, 2, half, ff), bf),
             pltpu.VMEM((GROUP, 2, half, d_model), bf),
             pltpu.VMEM((GROUP, half, d_model), bf),
             pltpu.VMEM((GROUP, half, d_model), bf),
@@ -641,7 +684,7 @@
             dma((7, GROUP)), dma((7, GROUP)), dma((6, GROUP, 3)), dma((6, GROUP, 3)), dma((7,)),
             dma((2,)),
             dma((GROUP,)), dma((GROUP,)), dma, dma,
-            dma((2,)), dma((GROUP,)), dma((GROUP,)), dma((GROUP,)), dma((GROUP,)),
+            dma((2, 2)), dma((GROUP, 2)), dma((GROUP, 2)), dma((GROUP, 2)), dma((GROUP, 2)),
             dma((GROUP, GROUP)), dma((GROUP, GROUP)), dma((GROUP, GROUP)), dma((2, GROUP)),
             dma((2, GROUP)),
         ],

time: 157 us -> 149 us (0.949); the launches traced: 155 us -> 149 us
  Pallas kernels: 153 us -> 147 us
    pallas_call x1, Pallas kernels: 153 us -> 147 us  [grouped(): pl.pallas_call(layer_kernel, out_shape=jax.ShapeDtypeStruct(resid.shape,...]
where the time goes in v3:
time: 149 us
  Pallas kernels  147 us (99%)
  local copies, waits for them, and re-layouts  1.88 us (1%)
    pallas_call x1, Pallas kernels, grouped(): pl.pallas_call(layer_kernel, out_shape=jax.ShapeDtypeStruct(resid.shape,...  147 us

profile of v3, /device:TPU:0, one launch (start us, length us, event | category | flops | bytes accessed | tf_op | source)
XLA Modules:
  0.0 149.0 jit_solution(4718037361409753925)
XLA Ops:
  0.0 147.1 %shard_map.118 = bf16[128,2048]{1,0:T(8,128)(2,1)} custom-call(bf16[256,1024]{1,0:T(8,128)(2,1)} %q_ref.1, bf16[256,512]{1,0:T(8,128)(2,1)} %k_ref.1, bf16[256,512]{1,0:T(8,128)(2,1)} %v_ref.1, s32[1,256]{1,0:T(1,128)} %bitcast.5, f32[8,4096]{1,0:T(8,128)} %lg_ref.1, bf16[1024,2048]{1,0:T(8,128)(2,1)} %ow_hbm.1, bf16[128,2048]{1,0:T(8,128)(2,1)} %resid_hbm.1, ...), custom_call_target="tpu_custom_call" | custom-call | tf_op jit(solution)/shard_map/pallas_call | solution.py:656
  147.1 1.9 %copy.14 = bf16[128,2048]{1,0:T(8,128)(2,1)} copy(bf16[128,2048]{1,0:T(8,128)(2,1)} %shard_map.118) | data formatting | bytes 1048576

commit v4 on v3

--- a/solution.py
+++ b/solution.py
@@ -339,6 +339,7 @@
         @pl.when(zq == GROUP - 1)
         def _():
             forwards(GATE)
+            z_sends(DOWN)
 
         @pl.when(zq != z)
         def _():
@@ -395,7 +396,6 @@
         def _():
             remote(att.at[zq], arr.at[z], a_send.at[zq], a_recv.at[z], there(zq)).start()
 
-    z_sends(DOWN)
     forwards(UP)
     spread_own(DOWN)
     for load in loads:
@@ -543,27 +543,29 @@
 
     @pl.loop(0, 2)
     def _(c):
-        expand(z, c)
+        expand(mate_z, c)
         arrive(2, c)
 
-    @pl.loop(0, 2)
-    def _(c):
-        expand(mate_z, c)
-
-    @pl.loop(0, GROUP)
-    def _(g):
-        at = span(g, gcols)
-        for e in neighbours:
-            p_arrival(DOWN, g, e)
-        lower(mate_z, g)
-        lower(z, g)
-        trade(mate_z, g).wait()
-        red[mate_z, :, at] = both(mate_z, at).astype(jnp.bfloat16)
-        give(mate_z, g).start()
-        trade(z, g).wait()
+    @pl.loop(0, GROUP + 1)
+    def _(s):
+        @pl.when(s < GROUP)
+        def _():
+            for e in neighbours:
+                p_arrival(DOWN, s, e)
+            lower(mate_z, s)
+
+        @pl.when(s > 0)
+        def _():
+            at = span(s - 1, gcols)
+            trade(mate_z, s - 1).wait()
+            red[mate_z, :, at] = both(mate_z, at).astype(jnp.bfloat16)
+            give(mate_z, s - 1).start()
+
+    def far_block(t):
+        return far + t + (1 - 2 * t) * (z // 2)
 
     def send_far(t):
-        zb = far + t + (1 - 2 * t) * (z // 2)
+        zb = far_block(t)
 
         @pl.loop(0, 2)
         def _(c):
@@ -586,6 +588,9 @@
                     red[zb, rs, cs] = both_far(zb, rs, cs).astype(jnp.bfloat16)
                     give_comb(t, zb, c, h).start()
 
+    def combine(t):
+        zb = far_block(t)
+
         @pl.when((z > 0) & (z < GROUP - 1))
         def _():
             @pl.loop(0, 2)
@@ -599,6 +604,21 @@
 
     send_far(0)
     send_far(1)
+    combine(0)
+
+    @pl.loop(0, 2)
+    def _(c):
+        expand(z, c)
+
+    @pl.loop(0, GROUP)
+    def _(g):
+        lower(z, g)
+
+    combine(1)
+
+    @pl.loop(0, GROUP)
+    def _(g):
+        trade(z, g).wait()
 
     for c in (0, 1):
         for h in (0, 1):

time: 149 us -> 148 us (level)
    pallas_call x1, Pallas kernels: 147 us -> 146 us  [grouped(): pl.pallas_call(layer_kernel, out_shape=jax.ShapeDtypeStruct(resid.shape,...]
where the time goes in v4:
time: 148 us; the launch traced here: 147 us
  Pallas kernels  146 us (99%)
  local copies, waits for them, and re-layouts  1.88 us (1%)
    pallas_call x1, Pallas kernels, grouped(): pl.pallas_call(layer_kernel, out_shape=jax.ShapeDtypeStruct(resid.shape,...  146 us

profile of v4, /device:TPU:0, one launch (start us, length us, event | category | flops | bytes accessed | tf_op | source)
XLA Modules:
  0.0 147.4 jit_solution(5094708072211546868)
XLA Ops:
  0.0 145.5 %shard_map.118 = bf16[128,2048]{1,0:T(8,128)(2,1)} custom-call(bf16[256,1024]{1,0:T(8,128)(2,1)} %q_ref.1, bf16[256,512]{1,0:T(8,128)(2,1)} %k_ref.1, bf16[256,512]{1,0:T(8,128)(2,1)} %v_ref.1, s32[1,256]{1,0:T(1,128)} %bitcast.5, f32[8,4096]{1,0:T(8,128)} %lg_ref.1, bf16[1024,2048]{1,0:T(8,128)(2,1)} %ow_hbm.1, bf16[128,2048]{1,0:T(8,128)(2,1)} %resid_hbm.1, ...), custom_call_target="tpu_custom_call" | custom-call | tf_op jit(solution)/shard_map/pallas_call | solution.py:676
  145.5 1.9 %copy.14 = bf16[128,2048]{1,0:T(8,128)(2,1)} copy(bf16[128,2048]{1,0:T(8,128)(2,1)} %shard_map.118) | data formatting | bytes 1048576

commit v5 on v4

--- a/solution.py
+++ b/solution.py
@@ -235,6 +235,20 @@
     for e in neighbours:
         pl.semaphore_signal(barrier, inc=1, device_id=near(e), device_id_type=MESH)
     pl.semaphore_signal(barrier, inc=1, device_id=mate, device_id_type=MESH)
+    lanes = 128
+
+    def gate_row(r, at):
+        block = lg_ref[:, at]
+        chosen = lax.broadcasted_iota(jnp.int32, block.shape, 0) == z * rank + r
+        return jnp.sum(jnp.where(chosen, block, 0.0), axis=0, keepdims=True) * LOG2E
+
+    @pl.loop(0, kall.shape[0] // lanes)
+    def _(j):
+        at = span(j, lanes)
+        for r in range(rank):
+            row = gate_row(r, at)
+            gkc[r, at, :] = jnp.transpose(jnp.broadcast_to(row, (lanes, lanes)))
+
     pl.semaphore_wait(barrier, 7)
 
     def z_copy(a, to):
@@ -280,20 +294,6 @@
         own_copy(a).start()
     for load in loads:
         load.start()
-
-    lanes = 128
-
-    def gate_row(r, at):
-        block = lg_ref[:, at]
-        chosen = lax.broadcasted_iota(jnp.int32, block.shape, 0) == z * rank + r
-        return jnp.sum(jnp.where(chosen, block, 0.0), axis=0, keepdims=True) * LOG2E
-
-    @pl.loop(0, kall.shape[0] // lanes)
-    def _(j):
-        at = span(j, lanes)
-        for r in range(rank):
-            row = gate_row(r, at)
-            gkc[r, at, :] = jnp.transpose(jnp.broadcast_to(row, (lanes, lanes)))
 
     def ascending(i):
         return i + (i - z + GROUP) // GROUP

time: 148 us -> 149 us (level)
    pallas_call x1, Pallas kernels: 146 us -> 147 us  [grouped(): pl.pallas_call(layer_kernel, out_shape=jax.ShapeDtypeStruct(resid.shape,...]
where the time goes in v5:
time: 149 us
  Pallas kernels  147 us (99%)
  local copies, waits for them, and re-layouts  1.88 us (1%)
    pallas_call x1, Pallas kernels, grouped(): pl.pallas_call(layer_kernel, out_shape=jax.ShapeDtypeStruct(resid.shape,...  147 us

profile of v5, /device:TPU:0, one launch (start us, length us, event | category | flops | bytes accessed | tf_op | source)
XLA Modules:
  0.0 149.2 jit_solution(6892023713393357920)
XLA Ops:
  0.0 147.3 %shard_map.118 = bf16[128,2048]{1,0:T(8,128)(2,1)} custom-call(bf16[256,1024]{1,0:T(8,128)(2,1)} %q_ref.1, bf16[256,512]{1,0:T(8,128)(2,1)} %k_ref.1, bf16[256,512]{1,0:T(8,128)(2,1)} %v_ref.1, s32[1,256]{1,0:T(1,128)} %bitcast.5, f32[8,4096]{1,0:T(8,128)} %lg_ref.1, bf16[1024,2048]{1,0:T(8,128)(2,1)} %ow_hbm.1, bf16[128,2048]{1,0:T(8,128)(2,1)} %resid_hbm.1, ...), custom_call_target="tpu_custom_call" | custom-call | tf_op jit(solution)/shard_map/pallas_call | solution.py:676
  147.3 1.9 %copy.14 = bf16[128,2048]{1,0:T(8,128)(2,1)} copy(bf16[128,2048]{1,0:T(8,128)(2,1)} %shard_map.118) | data formatting | bytes 1048576
